TPU v7x, 32 devices: a whole 2x2x4 slice. The times are simulated.
32 devices in a mesh: ep: 8 (over z, x), tp: 4 (over y, core).
Axes of the slice: x: 2, y: 2, z: 4, core: 2. Of those that a mesh axis runs over, the one named last changes fastest.
Arguments:
- tokens: bfloat16 [6144, 2048], P(('ep', 'tp')), may hold values from -6 to 6
- routes: int32 [6144, 2], P(('ep', 'tp')), may hold values from 0 to 7, all different within a row; in each aligned block of 192 rows (0 to 191, 192 to 383, ...) at most 64 rows name the same one
- gates: float32 [6144, 2], P(('ep', 'tp')), may hold values from 0.3 to 2.2
- pre_gain: float32 [2048], replicated, may hold values from 0.1 to 1.9
- w_gate: bfloat16 [8, 2048, 512], P('ep'), may hold values from -0.125 to 0.125
- w_up: bfloat16 [8, 2048, 512], P('ep'), may hold values from -0.125 to 0.125
- w_down: bfloat16 [8, 512, 2048], P('ep'), may hold values from -0.25 to 0.25
- sh_gate: bfloat16 [2048, 512], P('tp'), may hold values from -0.125 to 0.125
- sh_up: bfloat16 [2048, 512], P('tp'), may hold values from -0.125 to 0.125
- sh_down: bfloat16 [512, 2048], P(None, 'tp'), may hold values from -0.25 to 0.25
- post_gain: float32 [2048], replicated, may hold values from 0.1 to 1.9
Outputs:
- mixed: bfloat16 [6144, 2048], P('ep', 'tp')
Inputs may be any that keep to these rules, and one draw needn't show every extreme that they name: `routes`: each token names 2 different experts; among the rows of one device no expert is named more than 64 times, a bound that some block reaches.
All inputs are finite; a program needn't handle non-finite values.
Results may differ from a plain program's by a relative error of at most 0.0075.
Values may be sent and summed in bfloat16 or wider, within the bound.
A program may use at most 64 MiB of HBM per device.

v0:
```python
import jax
import jax.numpy as jnp
from jax import lax
from jax.sharding import PartitionSpec as P

TOPK = 2


def per_device(
    tokens, routes, gates, pre_gain, w_gate, w_up, w_down, sh_gate, sh_up, sh_down, post_gain
):
    tok_rows, full_width = tokens.shape
    experts_all = lax.axis_size("ep")
    capacity = max(2, 4 * tok_rows * TOPK // (3 * experts_all))
    inputs = tokens.astype(jnp.float32)
    scale_in = lax.rsqrt(jnp.mean(inputs * inputs, axis=1, keepdims=True) + 1e-06)
    normed = (inputs * scale_in * pre_gain[None, :]).astype(jnp.bfloat16)
    gate_shared = jnp.dot(
        normed,
        lax.all_gather(sh_gate, "tp", axis=0, tiled=True),
        preferred_element_type=jnp.float32,
    )
    up_shared = jnp.dot(
        normed, lax.all_gather(sh_up, "tp", axis=0, tiled=True), preferred_element_type=jnp.float32
    )
    shared_hidden = (jax.nn.silu(gate_shared) * up_shared).astype(jnp.bfloat16)
    pair_count = tok_rows * TOPK
    expert_ids = routes.reshape(pair_count)
    matches = (expert_ids[:, None] == jnp.arange(experts_all, dtype=jnp.int32)[None, :]).astype(
        jnp.int32
    )
    earlier = jnp.cumsum(matches, axis=0) - matches
    slot_index = jnp.sum(earlier * matches, axis=1)
    dest_slot = expert_ids * capacity + slot_index
    pair_token = jnp.arange(pair_count, dtype=jnp.int32) // TOPK
    slot_token = (
        jnp.full((experts_all * capacity,), tok_rows, jnp.int32).at[dest_slot].set(pair_token)
    )
    padded = jnp.concatenate([normed, jnp.zeros((1, full_width), jnp.bfloat16)], axis=0)
    outgoing = padded[slot_token].reshape(experts_all, capacity, full_width)
    arrived = lax.all_to_all(outgoing, "ep", split_axis=0, concat_axis=0, tiled=True)
    sources, count, width_in = arrived.shape
    flat_rows = arrived.reshape(sources * count, width_in)
    gate_part = jnp.dot(flat_rows, w_gate[0], preferred_element_type=jnp.float32)
    up_part = jnp.dot(flat_rows, w_up[0], preferred_element_type=jnp.float32)
    hidden = (jax.nn.silu(gate_part) * up_part).astype(jnp.bfloat16)
    result = jnp.dot(hidden, w_down[0], preferred_element_type=jnp.float32).astype(jnp.bfloat16)
    returned = lax.all_to_all(
        result.reshape(sources, count, width_in), "ep", split_axis=0, concat_axis=0, tiled=True
    )
    picked = returned.reshape(experts_all * capacity, full_width)[dest_slot]
    weighted = picked.astype(jnp.float32) * gates.reshape(pair_count)[:, None]
    routed = jnp.sum(weighted.reshape(tok_rows, TOPK, full_width), axis=1).astype(jnp.bfloat16)
    shared = jnp.dot(
        shared_hidden,
        lax.all_gather(sh_down, "tp", axis=1, tiled=True),
        preferred_element_type=jnp.float32,
    ).astype(jnp.bfloat16)
    combined = routed.astype(jnp.float32) + shared.astype(jnp.float32)
    scale_out = lax.rsqrt(jnp.mean(combined * combined, axis=1, keepdims=True) + 1e-06)
    out_rows = (combined * scale_out * post_gain[None, :]).astype(jnp.bfloat16)
    return lax.all_to_all(out_rows, "tp", split_axis=1, concat_axis=0, tiled=True)


def solution(mesh):
    return jax.shard_map(
        per_device,
        mesh=mesh,
        in_specs=(
            P(("ep", "tp"), None),
            P(("ep", "tp"), None),
            P(("ep", "tp"), None),
            P(),
            P("ep", None, None),
            P("ep", None, None),
            P("ep", None, None),
            P("tp", None),
            P("tp", None),
            P(None, "tp"),
            P(),
        ),
        out_specs=P("ep", "tp"),
        check_vma=False,
    )
```

profile of v0, /device:TPU:0, one launch (start us, length us, event | category | flops | bytes accessed | tf_op | source)
XLA Modules:
  0.0 186.4 jit_solution(4112277381100023838)
XLA Ops:
  6.5 0.7 all-gather.4.cloned.1.call-update
  7.3 0.8 copy.20
  8.1 0.1 eq.29
  8.2 0.1 eq.25
  8.4 0.7 broadcast_multiply_fusion
  9.1 0.8 reduce-window.6
  9.9 0.2 slice_reduce_fusion
  10.2 0.1 copy.19
  10.3 0.1 mul.87
  10.4 1.4 fusion.7
  11.8 0.9 fusion.9
  12.8 0.9 copy-done.1
  13.9 2.9 %scatter_custom_fusion = s32[512]{0:T(512)S(1)} fusion(s32[384]{0:T(512)S(1)} %fusion.32, s32[384]{0:T(512)S(1)} %add_select_fusion, s32[]{:T(128)} %constant.38.clone.1), kind=kCustom, calls=%fused_computation.53 | custom fusion | bytes 2052 | tf_op jit(solution)/shard_map/scatter | solution.py:37
  16.8 3.3 %gather_fusion = bf16[512,2048]{1,0:T(8,128)(2,1)} fusion(bf16[193,2048]{1,0:T(8,128)(2,1)S(1)} %concatenate.3, s32[1024]{0:T(1024)S(1)} %pad_clamp_fusion.1), kind=kCustom, calls=%fused_computation | custom fusion | bytes 4196352 | tf_op jit(solution)/shard_map/gather | solution.py:40
  20.1 7.3 %all-to-all-start = ((bf16[8,64,2048]{2,1,0:T(8,128)(2,1)}), bf16[8,64,2048]{2,1,0:T(8,128)(2,1)}, u32[]{:S(2)}, u32[]{:S(2)}) async-start(bf16[8,64,2048]{2,1,0:T(8,128)(2,1)} %bitcast.42), calls=%async_computation | async-start | bytes 4194304 | tf_op jit(solution)/shard_map/all_to_all | solution.py:41
  27.4 0.7 all-gather.6.cloned.1.call-update
  28.1 47.6 %all-to-all-done = bf16[8,64,2048]{2,1,0:T(8,128)(2,1)} async-done(((bf16[8,64,2048]{2,1,0:T(8,128)(2,1)}), bf16[8,64,2048]{2,1,0:T(8,128)(2,1)}, u32[]{:S(2)}, u32[]{:S(2)}) %all-to-all-start) | async-done | bytes 2097184 | tf_op jit(solution)/shard_map/all_to_all | solution.py:41
  75.7 4.5 %fusion.5 = f32[512,512]{1,0:T(8,128)} fusion(bf16[512,2048]{1,0:T(8,128)(2,1)} %bitcast.3, bf16[1,2048,512]{2,1,0:T(8,128)(2,1)} %param.15), kind=kOutput, calls=%fused_computation.11 | convolution fusion | flops 1073741824 | bytes 5242880 | tf_op jit(solution)/shard_map/dot_general | solution.py:44
  80.3 6.3 %convolution_convert_fusion = bf16[512,2048]{1,0:T(8,128)(2,1)} fusion(bf16[1,512,2048]{2,1,0:T(8,128)(2,1)S(1)} %copy-done, bf16[512,2048]{1,0:T(8,128)(2,1)} %bitcast.3, bf16[1,2048,512]{2,1,0:T(8,128)(2,1)} %param.16, f32[512,512]{1,0:T(8,128)} %fusion.5), kind=kOutput, calls=%fused_computation.4 | convolution fusion | flops 2150105088 | bytes 9437184 | tf_op jit(solution)/shard_map/dot_general | solution.py:47
  86.6 4.5 %all-to-all-start.1 = ((bf16[8,64,2048]{2,1,0:T(8,128)(2,1)}), bf16[8,64,2048]{2,1,0:T(8,128)(2,1)}, u32[]{:S(2)}, u32[]{:S(2)}) async-start(bf16[8,64,2048]{2,1,0:T(8,128)(2,1)} %bitcast.46), calls=%async_computation.1 | async-start | bytes 4194304 | tf_op jit(solution)/shard_map/all_to_all | solution.py:48
  91.1 0.2 all-gather.8.cloned.1.call-start
  91.3 0.5 all-gather.8.cloned.1.call-update
  91.9 0.1 copy.22
  92.0 2.2 %fusion.37 = f32[192,512]{1,0:T(8,128)S(1)} fusion(bf16[192,2048]{1,0:T(8,128)(2,1)S(1)} %copy-done.2, bf16[2048,512]{1,0:T(8,128)(2,1)} %all-gather.4.cloned.1.call-done), kind=kOutput, calls=%fused_computation.58 | convolution fusion | flops 402653184 | bytes 3276800 | tf_op jit(solution)/shard_map/dot_general | solution.py:18
  94.2 44.7 %all-to-all-done.1 = bf16[8,64,2048]{2,1,0:T(8,128)(2,1)} async-done(((bf16[8,64,2048]{2,1,0:T(8,128)(2,1)}), bf16[8,64,2048]{2,1,0:T(8,128)(2,1)}, u32[]{:S(2)}, u32[]{:S(2)}) %all-to-all-start.1) | async-done | bytes 2097184 | tf_op jit(solution)/shard_map/all_to_all | solution.py:48
  138.9 6.9 %gather_fusion.1 = bf16[384,2048]{1,0:T(8,128)(2,1)} fusion(bf16[512,2048]{1,0:T(8,128)(2,1)} %bitcast.8, s32[1024]{0:T(1024)S(1)} %pad_clamp_fusion), kind=kCustom, calls=%fused_computation.1 | custom fusion | bytes 3147264 | tf_op jit(solution)/shard_map/gather | solution.py:51
  145.8 4.8 %reshape.94 = f32[192,2,2048]{2,1,0:T(2,128)} reshape(bf16[384,2048]{1,0:T(8,128)(2,1)} %gather_fusion.1) | data formatting | bytes 4718592 | tf_op jit(solution)/shard_map/convert_element_type | solution.py:52
  150.6 7.8 %multiply_reduce_fusion = bf16[192,2048]{1,0:T(8,128)(2,1)} fusion(f32[192,2,2048]{2,1,0:T(2,128)} %reshape.94, f32[192,2]{1,0:T(8,128)S(1)} %copy.22), kind=kLoop, calls=%fused_computation.3 | loop fusion | flops 1179648 | bytes 3933696 | tf_op jit(solution)/shard_map/reduce_sum | solution.py:53
  158.4 4.7 %multiply_reduce_fusion.1 = (f32[192]{0:T(256)S(1)}, f32[192,2048]{1,0:T(8,128)}) fusion(bf16[512,2048]{1,0:T(8,128)(2,1)} %all-gather.8.cloned.1.call-done, bf16[192,2048]{1,0:T(8,128)(2,1)S(1)} %copy-done.2, bf16[2048,512]{1,0:T(8,128)(2,1)} %all-gather.6.cloned.1.call-done, f32[192,512]{1,0:T(8,128)S(1)} %fusion.37, ...), kind=kOutput, calls=%fused_computation.19 | convolution fusion | flops 808255296 | bytes 7734016 | tf_op jit(solution)/shard_map/dot_general | solution.py:54
  163.1 1.6 multiply_convert_fusion
  164.8 14.2 %all_to_all.29 = bf16[192,4,512]{2,0,1:T(8,128)(2,1)S(1)} all-to-all(bf16[192,4,512]{2,0,1:T(8,128)(2,1)S(1)} %bitcast.43), channel_id=1, replica_groups=mesh['ep'=8,'tp'=4] {'tp'}, dimensions={1} | all-to-all | bytes 1572864 | tf_op jit(solution)/shard_map/all_to_all | solution.py:62
  179.0 0.9 copy.28
  (28 shorter events, 0.4 us)
Async XLA Ops:
  6.5 73.7 %copy-start = (bf16[1,512,2048]{2,1,0:T(8,128)(2,1)S(1)}, bf16[1,512,2048]{2,1,0:T(8,128)(2,1)}, u32[]{:S(2)}) copy-start(bf16[1,512,2048]{2,1,0:T(8,128)(2,1)} %param.17) | copy-start | bytes 6291460
  6.5 5.3 %copy-start.3 = (bf16[192,2048]{1,0:T(8,128)(2,1)S(1)}, bf16[192,2048]{1,0:T(8,128)(2,1)}, u32[]{:S(2)}) copy-start(bf16[192,2048]{1,0:T(8,128)(2,1)} %param.11) | copy-start | bytes 2359300
  6.5 85.5 %all-gather.4.cloned.1.call-start = ((), (), s32[]{:S(2)}) async-start(), calls=%async_computation.3 | async-start | bytes 2621440 | tf_op jit(solution)/shard_map/all_gather | solution.py:20
  12.8 0.9 copy-start.1
  20.1 55.6 %all-to-all-start = ((bf16[8,64,2048]{2,1,0:T(8,128)(2,1)}), bf16[8,64,2048]{2,1,0:T(8,128)(2,1)}, u32[]{:S(2)}, u32[]{:S(2)}) async-start(bf16[8,64,2048]{2,1,0:T(8,128)(2,1)} %bitcast.42), calls=%async_computation | async-start | bytes 4194304 | tf_op jit(solution)/shard_map/all_to_all | solution.py:41
  27.4 131.0 %all-gather.6.cloned.1.call-start = ((), (), s32[]{:S(2)}) async-start(), calls=%async_computation.4 | async-start | bytes 2621440 | tf_op jit(solution)/shard_map/all_gather | solution.py:24
  86.6 5.2 %copy-start.5 = (f32[192,2]{0,1:T(2,128)S(1)}, f32[192,2]{0,1:T(2,128)}, u32[]{:S(2)}) copy-start(f32[192,2]{0,1:T(2,128)} %param.13) | copy-start | bytes 4612
  86.6 5.4 %copy-start.2 = (bf16[192,2048]{1,0:T(8,128)(2,1)S(1)}, bf16[192,2048]{1,0:T(8,128)(2,1)}, u32[]{:S(2)}) copy-start(bf16[192,2048]{1,0:T(8,128)(2,1)} %copy-done.1) | copy-start | bytes 2359300
  86.6 52.3 %all-to-all-start.1 = ((bf16[8,64,2048]{2,1,0:T(8,128)(2,1)}), bf16[8,64,2048]{2,1,0:T(8,128)(2,1)}, u32[]{:S(2)}, u32[]{:S(2)}) async-start(bf16[8,64,2048]{2,1,0:T(8,128)(2,1)} %bitcast.46), calls=%async_computation.1 | async-start | bytes 4194304 | tf_op jit(solution)/shard_map/all_to_all | solution.py:48
  91.1 67.3 %all-gather.8.cloned.1.call-start = ((), (), s32[]{:S(2)}) async-start(), calls=%async_computation.5 | async-start | bytes 2621440 | tf_op jit(solution)/shard_map/all_gather | solution.py:56
  158.4 4.7 %copy-start.4 = (f32[2048]{0:T(1024)S(1)}, f32[2048]{0:T(1024)}, u32[]{:S(2)}) copy-start(f32[2048]{0:T(1024)} %param.21) | copy-start | bytes 24580
Sparse Core Ops, SparseCore 0:
  8.9 25.3 all-gather.3
  35.8 22.5 all-gather.5
  93.5 23.8 all-gather.7
where the time goes:
time: 187 us; the launch traced here: 186 us
  waiting for transfers between devices  94.2 us (50%)
  local copies, waits for them, and re-layouts  21.5 us (11%)
  matrix products  17.7 us (9%)
  blocking collectives  14.2 us (8%)
  other arithmetic  13.4 us (7%)
  between operations  13.3 us (7%)
  starting transfers between devices  12 us (6%)
    all_to_all x1, waiting for transfers between devices, per_device(): lax.all_to_all(outgoing, 'ep', split_axis=0, concat_axis=0, tiled=True)  47.6 us
    all_to_all x1, waiting for transfers between devices, per_device(): lax.all_to_all(result.reshape(sources, count, width_in), 'ep', split_axis...  44.7 us
    all_to_all x1, blocking collectives, per_device(): lax.all_to_all(out_rows, 'tp', split_axis=1, concat_axis=0, tiled=True)  14.2 us
    reduce_sum x1, other arithmetic, per_device(): jnp.sum(weighted.reshape(tok_rows, TOPK, full_width), axis=1)  7.76 us
    all_to_all x1, starting transfers between devices, per_device(): lax.all_to_all(outgoing, 'ep', split_axis=0, concat_axis=0, tiled=True)  7.28 us
    gather x1, local copies, waits for them, and re-layouts, per_device(): picked = returned.reshape(experts_all * capacity, full_width)[dest_slot]  6.91 us
    dot_general x1, matrix products, per_device(): jnp.dot(hidden, w_down[0], preferred_element_type=jnp.float32)  6.33 us
    convert_element_type x1, local copies, waits for them, and re-layouts, per_device(): weighted = picked.astype(jnp.float32) * gates.reshape(pair_count)[:, None]  4.82 us
  transfers between devices with their start and end apart: 5, of which 2 were waited for; matrix products, arithmetic and copies ran while one was open for 24% of the time, Pallas kernels for 0%

commit v1 on v0

v1 whole, which is shorter than its diff:
```python
import functools

import jax
import jax.numpy as jnp
from jax import lax
from jax.experimental import pallas as pl
from jax.experimental.pallas import tpu as pltpu
from jax.sharding import PartitionSpec as P

TOPK = 2
F32 = jnp.float32
BF16 = jnp.bfloat16
MESH = pl.DeviceIdType.MESH


def silu(v):
    return v / (1.0 + jnp.exp(-v))


def dot(a, b):
    return jnp.dot(a, b, preferred_element_type=F32)


def kernel(
    n, tp, cap,
    tokens, routes, gates, pre_gain, post_gain, w_gate, w_up, w_down, sh_gate, sh_up, sh_down,
    out,
    normed, key, pick, send, recv, res, ret, wg, wu, wd, sg, su, sd, acc, shared, obuf,
    load_sem, d_send, d_recv, r_send, r_recv, s_send, s_recv, o_send, o_recv,
):
    rows, width = tokens.shape
    block = 32 if rows % 32 == 0 else rows
    cols = width // tp
    me = lax.axis_index("ep")
    mt = lax.axis_index("tp")
    half = n // 2
    mine = lax.rem(me, half)
    near = me - mine
    far = lax.rem(near + half, n)

    barrier = pltpu.get_barrier_semaphore()

    def greet_ep(k, c):
        pl.semaphore_signal(
            barrier, inc=1, device_id={"ep": lax.rem(me + k, n)}, device_id_type=MESH
        )
        return c

    def greet_tp(k, c):
        pl.semaphore_signal(
            barrier, inc=1, device_id={"tp": lax.rem(mt + k, tp)}, device_id_type=MESH
        )
        return c

    lax.fori_loop(1, n, greet_ep, 0)
    lax.fori_loop(1, tp, greet_tp, 0)

    loads = [
        pltpu.make_async_copy(src, dst, load_sem.at[i])
        for i, (src, dst) in enumerate(
            (
                (w_gate.at[0], wg),
                (w_up.at[0], wu),
                (w_down.at[0], wd),
                (sh_gate, sg.at[mt]),
                (sh_up, su.at[mt]),
                (sh_down, sd.at[mt]),
            )
        )
    ]
    for load in loads:
        load.start()

    def norm_rows(i, c):
        at = pl.ds(pl.multiple_of(i * block, block), block)
        v = tokens[at, :].astype(F32)
        scale = lax.rsqrt(jnp.mean(v * v, axis=1, keepdims=True) + 1e-06)
        normed[at, :] = (v * scale * pre_gain[...]).astype(BF16)
        return c

    lax.fori_loop(0, rows // block, norm_rows, 0)

    lanes = key.shape[0]
    expert = lax.broadcasted_iota(jnp.int32, (rows, lanes), 1)
    named = (routes[:, 0:1] == expert) | (routes[:, 1:2] == expert)
    named = jnp.where(named, 1.0, 0.0).astype(BF16)
    row = lax.broadcasted_iota(jnp.int32, (rows, rows), 0)
    column = lax.broadcasted_iota(jnp.int32, (rows, rows), 1)
    before = jnp.where(row < column, 1.0, 0.0).astype(BF16)
    same = jnp.where(row == column, 1.0, 0.0).astype(BF16)
    over_rows = (((0,), (0,)), ((), ()))
    rank = lax.dot_general(named, before, over_rows, preferred_element_type=F32)
    named_t = lax.dot_general(named, same, over_rows, preferred_element_type=F32)
    key[...] = jnp.where(named_t > 0.5, rank, -1.0)
    slot = lax.broadcasted_iota(jnp.int32, (cap, rows), 0).astype(F32)

    def fill(d):
        chosen = jnp.where(slot == key[pl.ds(d, 1), :], 1.0, 0.0).astype(BF16)
        pick[d] = chosen
        send[d] = dot(chosen, normed[...]).astype(BF16)

    def dispatch(d, s):
        return pltpu.make_async_remote_copy(
            src_ref=send.at[d], dst_ref=recv.at[s],
            send_sem=d_send.at[d], recv_sem=d_recv.at[s],
            device_id={"ep": d}, device_id_type=MESH,
        )

    def giveback(s, e):
        return pltpu.make_async_remote_copy(
            src_ref=res.at[s], dst_ref=ret.at[e],
            send_sem=r_send.at[s], recv_sem=r_recv.at[e],
            device_id={"ep": s}, device_id_type=MESH,
        )

    def share(which, d, s):
        src, dst = ((sh_gate, sg), (sh_up, su), (sh_down, sd))[which]
        return pltpu.make_async_remote_copy(
            src_ref=src, dst_ref=dst.at[s],
            send_sem=s_send.at[which, d], recv_sem=s_recv.at[which, s],
            device_id={"tp": d}, device_id_type=MESH,
        )

    def emit(d, s):
        return pltpu.make_async_remote_copy(
            src_ref=obuf.at[d], dst_ref=out.at[pl.ds(pl.multiple_of(s * rows, rows), rows), :],
            send_sem=o_send.at[d], recv_sem=o_recv.at[s],
            device_id={"tp": d}, device_id_type=MESH,
        )

    fill(far + mine)
    pl.semaphore_wait(barrier, n - 1 + tp - 1)
    dispatch(far + mine, me).start()

    def send_far(j, c):
        d = far + lax.rem(mine + j, half)
        fill(d)
        dispatch(d, me).start()
        return c

    def send_near(j, c):
        d = near + lax.rem(mine + j, half)
        fill(d)
        dispatch(d, me).start()
        return c

    lax.fori_loop(1, half, send_far, 0)
    for which in range(3):
        def send_shared(k, c):
            share(which, lax.rem(mt + k, tp), mt).start()
            return c

        lax.fori_loop(1, tp, send_shared, 0)
    lax.fori_loop(1, half, send_near, 0)
    fill(me)

    for load in loads[:3]:
        load.wait()

    def run(x):
        hidden = (silu(dot(x, wg[...])) * dot(x, wu[...])).astype(BF16)
        return dot(hidden, wd[...]).astype(BF16)

    ret[me] = run(send[me])

    def serve(s):
        dispatch(me, s).wait_recv()
        res[s] = run(recv[s])
        giveback(s, me).start()

    def serve_far(j, c):
        serve(far + lax.rem(mine + half - j, half))
        return c

    def serve_near(j, c):
        serve(near + lax.rem(mine + half - j, half))
        return c

    lax.fori_loop(0, half, serve_far, 0)
    lax.fori_loop(1, half, serve_near, 0)

    def weight_of(e):
        first = jnp.where(routes[:, 0:1] == e, gates[:, 0:1], 0.0)
        return first + jnp.where(routes[:, 1:2] == e, gates[:, 1:2], 0.0)

    def placed(e):
        rowsof = lax.dot_general(pick[e], ret[e], over_rows, preferred_element_type=F32)
        return weight_of(e) * rowsof

    acc[...] = placed(me)

    for load in loads[3:]:
        load.wait()

    def arrive(which):
        def one(k, c):
            share(which, mt, lax.rem(mt + tp - k, tp)).wait_recv()
            return c

        lax.fori_loop(1, tp, one, 0)

    arrive(0)
    arrive(1)
    full = (width, sg.shape[2])
    gate_shared = dot(normed[...], sg[...].reshape(full))
    up_shared = dot(normed[...], su[...].reshape(full))
    shared_hidden = (silu(gate_shared) * up_shared).astype(BF16)
    arrive(2)

    def project(t, c):
        at = pl.ds(pl.multiple_of(t * cols, cols), cols)
        shared[:, at] = dot(shared_hidden, sd[t]).astype(BF16)
        return c

    lax.fori_loop(0, tp, project, 0)

    def gather_far(j, c):
        e = far + lax.rem(mine + j, half)
        giveback(me, e).wait_recv()
        acc[...] += placed(e)
        return c

    def gather_near(j, c):
        e = near + lax.rem(mine + j, half)
        giveback(me, e).wait_recv()
        acc[...] += placed(e)
        return c

    lax.fori_loop(1, half, gather_near, 0)
    lax.fori_loop(0, half, gather_far, 0)

    def finish(i, c):
        at = pl.ds(pl.multiple_of(i * block, block), block)
        combined = acc[at, :].astype(BF16).astype(F32) + shared[at, :].astype(F32)
        scale = lax.rsqrt(jnp.mean(combined * combined, axis=1, keepdims=True) + 1e-06)
        mixed = (combined * scale * post_gain[...]).astype(BF16)
        for t in range(tp):
            obuf[t, at, :] = mixed[:, t * cols : (t + 1) * cols]
        return c

    lax.fori_loop(0, rows // block, finish, 0)

    def send_out(k, c):
        emit(lax.rem(mt + k, tp), mt).start()
        return c

    lax.fori_loop(1, tp, send_out, 0)
    out[pl.ds(pl.multiple_of(mt * rows, rows), rows), :] = obuf[mt]

    def drain_far(j, c):
        d = far + lax.rem(mine + j, half)
        dispatch(d, me).wait_send()
        giveback(d, me).wait_send()
        return c

    def drain_near(j, c):
        d = near + lax.rem(mine + j, half)
        dispatch(d, me).wait_send()
        giveback(d, me).wait_send()
        return c

    lax.fori_loop(0, half, drain_far, 0)
    lax.fori_loop(1, half, drain_near, 0)

    def drain_tp(k, c):
        d = lax.rem(mt + k, tp)
        for which in range(3):
            share(which, d, mt).wait_send()
        emit(d, mt).wait_send()
        emit(mt, d).wait_recv()
        return c

    lax.fori_loop(1, tp, drain_tp, 0)


def per_device(
    tokens, routes, gates, pre_gain, w_gate, w_up, w_down, sh_gate, sh_up, sh_down, post_gain
):
    rows, width = tokens.shape
    n = lax.axis_size("ep")
    tp = lax.axis_size("tp")
    cap = -(-max(2, 4 * rows * TOPK // (3 * n)) // 16) * 16
    lanes = -(-n // 128) * 128
    hidden = w_gate.shape[2]
    sh = sh_gate.shape[1]
    cols = width // tp
    vmem = pl.BlockSpec(memory_space=pltpu.VMEM)
    hbm = pl.BlockSpec(memory_space=pl.ANY)
    dma = pltpu.SemaphoreType.DMA
    return pl.pallas_call(
        functools.partial(kernel, n, tp, cap),
        out_shape=jax.ShapeDtypeStruct((tp * rows, cols), BF16),
        in_specs=[vmem] * 5 + [hbm] * 6,
        out_specs=vmem,
        scratch_shapes=[
            pltpu.VMEM((rows, width), BF16),
            pltpu.VMEM((lanes, rows), F32),
            pltpu.VMEM((n, cap, rows), BF16),
            pltpu.VMEM((n, cap, width), BF16),
            pltpu.VMEM((n, cap, width), BF16),
            pltpu.VMEM((n, cap, width), BF16),
            pltpu.VMEM((n, cap, width), BF16),
            pltpu.VMEM((width, hidden), BF16),
            pltpu.VMEM((width, hidden), BF16),
            pltpu.VMEM((hidden, width), BF16),
            pltpu.VMEM((tp, width // tp, sh), BF16),
            pltpu.VMEM((tp, width // tp, sh), BF16),
            pltpu.VMEM((tp, sh, cols), BF16),
            pltpu.VMEM((rows, width), F32),
            pltpu.VMEM((rows, width), BF16),
            pltpu.VMEM((tp, rows, cols), BF16),
            dma((6,)),
            dma((n,)), dma((n,)), dma((n,)), dma((n,)),
            dma((3, tp)), dma((3, tp)),
            dma((tp,)), dma((tp,)),
        ],
        compiler_params=pltpu.CompilerParams(
            collective_id=0, has_side_effects=True, vmem_limit_bytes=56 * 1024 * 1024
        ),
    )(
        tokens, routes, gates, pre_gain.reshape(1, width), post_gain.reshape(1, width),
        w_gate, w_up, w_down, sh_gate, sh_up, sh_down,
    )


def solution(mesh):
    return jax.shard_map(
        per_device,
        mesh=mesh,
        in_specs=(
            P(("ep", "tp"), None),
            P(("ep", "tp"), None),
            P(("ep", "tp"), None),
            P(),
            P("ep", None, None),
            P("ep", None, None),
            P("ep", None, None),
            P("tp", None),
            P("tp", None),
            P(None, "tp"),
            P(),
        ),
        out_specs=P("ep", "tp"),
        check_vma=False,
    )
```

time: 187 us -> 119 us (0.64)
  Pallas kernels: 0 us -> 113 us
  waiting for transfers between devices: 94.2 us -> 0 us
  matrix products: 17.7 us -> 0 us
  local copies, waits for them, and re-layouts: 21.5 us -> 4.94 us
  blocking collectives: 14.2 us -> 0 us
  other arithmetic: 13.4 us -> 0 us
  between operations: 13.3 us -> 0.01 us
  starting transfers between devices: 12 us -> 0 us
    pallas_call x0 -> x1, Pallas kernels: none -> 113 us  [per_device(): pl.pallas_call(functools.partial(kernel, n, tp, cap), out_shape=jax.Shape...]
    all_to_all x2 -> x0, waiting for transfers between devices: 92.3 us -> none  [the longest x1 47.6 us: per_device(): lax.all_to_all(outgoing, 'ep', split_axis=0, concat_axis=0, tiled=True)]
    dot_general x4 -> x0, matrix products: 17.7 us -> none  [the longest x1 6.33 us: per_device(): jnp.dot(hidden, w_down[0], preferred_element_type=jnp.float32)]
    all_to_all x1 -> x0, blocking collectives: 14.2 us -> none  [per_device(): lax.all_to_all(out_rows, 'tp', split_axis=1, concat_axis=0, tiled=True)]
    all_to_all x2 -> x0, starting transfers between devices: 11.8 us -> none  [the longest x1 7.28 us: per_device(): lax.all_to_all(outgoing, 'ep', split_axis=0, concat_axis=0, tiled=True)]
    gather x2 -> x0, local copies, waits for them, and re-layouts: 10.2 us -> none  [the longest x1 6.91 us: per_device(): picked = returned.reshape(experts_all * capacity, full_width)[dest_slot]]
    reduce_sum x3 -> x0, other arithmetic: 9.22 us -> none  [the longest x1 7.76 us: per_device(): jnp.sum(weighted.reshape(tok_rows, TOPK, full_width), axis=1)]
    convert_element_type x1 -> x0, local copies, waits for them, and re-layouts: 4.82 us -> none  [per_device(): weighted = picked.astype(jnp.float32) * gates.reshape(pair_count)[:, None]]
  transfers between devices with their start and end apart: 5 -> 0, of which waited for: 2 -> 0; matrix products, arithmetic and copies ran while one was open for 24% -> 0% of each run, Pallas kernels for 0% -> 0%
where the time goes in v1:
time: 119 us; the launch traced here: 118 us
  Pallas kernels  113 us (95%)
  local copies, waits for them, and re-layouts  4.94 us (4%)
    pallas_call x1, Pallas kernels, per_device(): pl.pallas_call(functools.partial(kernel, n, tp, cap), out_shape=jax.Shape...  113 us
    unnamed x3, local copies, waits for them, and re-layouts  4.94 us

profile of v1, /device:TPU:0, one launch (start us, length us, event | category | flops | bytes accessed | tf_op | source)
XLA Modules:
  0.0 117.8 jit_solution(10790489329197394910)
XLA Ops:
  0.0 1.4 %copy.12.routes = s32[192,2]{1,0:T(8,128)} copy(s32[192,2]{0,1:T(2,128)} %param.12) | data formatting | bytes 3072 | tf_op args[1]
  1.4 1.4 %copy.13.gates = f32[192,2]{1,0:T(8,128)} copy(f32[192,2]{0,1:T(2,128)} %param.13) | data formatting | bytes 3072 | tf_op args[2]
  2.9 112.9 %shard_map.109 = bf16[768,512]{1,0:T(8,128)(2,1)} custom-call(bf16[192,2048]{1,0:T(8,128)(2,1)} %tokens.1, s32[192,2]{1,0:T(8,128)} %copy.12.routes, f32[192,2]{1,0:T(8,128)} %copy.13.gates, f32[1,2048]{1,0:T(1,128)} %bitcast.2, f32[1,2048]{1,0:T(1,128)} %bitcast.3, bf16[1,2048,512]{2,1,0:T(8,128)(2,1)} %w_gate.1, bf16[1,2048,512]{2,1,0:T(8,128)(2,1)} %w_up.1, ...), custom_call_target="tpu_custom_call" | custom-call | tf_op jit(solution)/shard_map/pallas_call | solution.py:290
  115.8 2.1 %copy.15 = bf16[768,512]{1,0:T(8,128)(2,1)} copy(bf16[768,512]{1,0:T(8,128)(2,1)} %shard_map.109) | data formatting | bytes 1572864

commit v2 on v1

v2 whole, which is shorter than its diff:
```python
import functools

import jax
import jax.numpy as jnp
from jax import lax
from jax.experimental import pallas as pl
from jax.experimental.pallas import tpu as pltpu
from jax.sharding import PartitionSpec as P

TOPK = 2
F32 = jnp.float32
BF16 = jnp.bfloat16
MESH = pl.DeviceIdType.MESH


def silu(v):
    return v / (1.0 + jnp.exp(-v))


def dot(a, b):
    return jnp.dot(a, b, preferred_element_type=F32)


def kernel(
    n, tp, cap,
    tokens, routes, gates, pre_gain, post_gain, w_gate, w_up, w_down, sh_gate, sh_up, sh_down,
    out,
    normed, key, pick, send, recv, res, ret, wg, wu, wd, sg, su, sd, acc, shared,
    routes_all, gates_all, hidden_all, sums,
    load_sem, d_send, d_recv, r_send, r_recv, s_send, s_recv,
):
    rows, width = tokens.shape
    block = 32 if rows % 32 == 0 else rows
    cols = width // tp
    me = lax.axis_index("ep")
    mt = lax.axis_index("tp")
    half = n // 2
    mine = lax.rem(me, half)
    near = me - mine
    far = lax.rem(near + half, n)

    barrier = pltpu.get_barrier_semaphore()

    def greet(k, c):
        flat = lax.rem(me * tp + mt + k, n * tp)
        pl.semaphore_signal(
            barrier, inc=1, device_id={"ep": flat // tp, "tp": lax.rem(flat, tp)},
            device_id_type=MESH,
        )
        return c

    lax.fori_loop(1, n * tp, greet, 0)

    loads = [
        pltpu.make_async_copy(src, dst, load_sem.at[i])
        for i, (src, dst) in enumerate(
            (
                (w_gate.at[0], wg),
                (w_up.at[0], wu),
                (w_down.at[0], wd),
                (sh_gate, sg.at[mt]),
                (sh_up, su.at[mt]),
                (sh_down, sd),
            )
        )
    ]
    for load in loads:
        load.start()

    def norm_rows(i, c):
        at = pl.ds(pl.multiple_of(i * block, block), block)
        v = tokens[at, :].astype(F32)
        scale = lax.rsqrt(jnp.mean(v * v, axis=1, keepdims=True) + 1e-06)
        normed[at, :] = (v * scale * pre_gain[...]).astype(BF16)
        return c

    lax.fori_loop(0, rows // block, norm_rows, 0)

    lanes = key.shape[1]
    row = lax.broadcasted_iota(jnp.int32, (rows, rows), 0)
    column = lax.broadcasted_iota(jnp.int32, (rows, rows), 1)
    before = jnp.where(row < column, 1.0, 0.0).astype(BF16)
    same = jnp.where(row == column, 1.0, 0.0).astype(BF16)
    over_rows = (((0,), (0,)), ((), ()))
    slot = lax.broadcasted_iota(jnp.int32, (cap, rows), 0).astype(F32)

    def index(t):
        expert = lax.broadcasted_iota(jnp.int32, (rows, lanes), 1)
        ids = routes_all[t]
        named = (ids[:, 0:1] == expert) | (ids[:, 1:2] == expert)
        named = jnp.where(named, 1.0, 0.0).astype(BF16)
        rank = lax.dot_general(named, before, over_rows, preferred_element_type=F32)
        named_t = lax.dot_general(named, same, over_rows, preferred_element_type=F32)
        key[t] = jnp.where(named_t > 0.5, rank, -1.0)

    def choose(t, e):
        chosen = jnp.where(slot == key[t, pl.ds(e, 1), :], 1.0, 0.0).astype(BF16)
        pick[t, e] = chosen
        return chosen

    routes_all[mt] = routes[...]
    gates_all[mt] = gates[...]
    index(mt)

    def fill(d):
        send[d] = dot(choose(mt, d), normed[...]).astype(BF16)

    def dispatch(d, s):
        return pltpu.make_async_remote_copy(
            src_ref=send.at[d], dst_ref=recv.at[s],
            send_sem=d_send.at[d], recv_sem=d_recv.at[s],
            device_id={"ep": d}, device_id_type=MESH,
        )

    def giveback(s, t, e, u):
        return pltpu.make_async_remote_copy(
            src_ref=res.at[s, t], dst_ref=ret.at[e, u],
            send_sem=r_send.at[s, t], recv_sem=r_recv.at[e, u],
            device_id={"ep": s, "tp": t}, device_id_type=MESH,
        )

    def share(which, d, s):
        src, dst = (
            (sh_gate, sg.at[s]),
            (sh_up, su.at[s]),
            (hidden_all.at[mt], hidden_all.at[s]),
            (routes, routes_all.at[s]),
            (gates, gates_all.at[s]),
            (sums.at[mt], sums.at[s]),
        )[which]
        return pltpu.make_async_remote_copy(
            src_ref=src, dst_ref=dst,
            send_sem=s_send.at[which, d], recv_sem=s_recv.at[which, s],
            device_id={"tp": d}, device_id_type=MESH,
        )

    def spread(which):
        def one(k, c):
            share(which, lax.rem(mt + k, tp), mt).start()
            return c

        lax.fori_loop(1, tp, one, 0)

    def arrive(which):
        def one(k, c):
            share(which, mt, lax.rem(mt + tp - k, tp)).wait_recv()
            return c

        lax.fori_loop(1, tp, one, 0)

    fill(far + mine)
    pl.semaphore_wait(barrier, n * tp - 1)
    dispatch(far + mine, me).start()

    def send_far(j, c):
        d = far + lax.rem(mine + j, half)
        fill(d)
        dispatch(d, me).start()
        return c

    def send_near(j, c):
        d = near + lax.rem(mine + j, half)
        fill(d)
        dispatch(d, me).start()
        return c

    lax.fori_loop(1, half, send_far, 0)
    spread(3)
    spread(4)
    spread(0)
    spread(1)
    lax.fori_loop(1, half, send_near, 0)
    fill(me)

    for load in loads[:3]:
        load.wait()

    def run(x):
        hidden = (silu(dot(x, wg[...])) * dot(x, wu[...])).astype(BF16)
        return dot(hidden, wd[...]).astype(BF16)

    def split(s, result):
        for t in range(tp):
            res[s, t] = result[:, t * cols : (t + 1) * cols]

    def send_back(s, first):
        def one(k, c):
            giveback(s, lax.rem(mt + k, tp), me, mt).start()
            return c

        lax.fori_loop(first, tp, one, 0)

    split(me, run(send[me]))
    send_back(me, 1)
    ret[me, mt] = res[me, mt]

    arrive(3)
    arrive(4)

    def index_other(k, c):
        t = lax.rem(mt + k, tp)
        index(t)

        def each(e, c):
            choose(t, e)
            return c

        lax.fori_loop(0, n, each, 0)
        return c

    lax.fori_loop(1, tp, index_other, 0)

    def serve(s):
        dispatch(me, s).wait_recv()
        split(s, run(recv[s]))
        send_back(s, 0)

    def serve_far(j, c):
        serve(far + lax.rem(mine + half - j, half))
        return c

    def serve_near(j, c):
        serve(near + lax.rem(mine + half - j, half))
        return c

    lax.fori_loop(0, half, serve_far, 0)
    lax.fori_loop(1, half, serve_near, 0)

    for load in loads[3:]:
        load.wait()
    arrive(0)
    arrive(1)
    full = (width, sg.shape[2])
    gate_shared = dot(normed[...], sg[...].reshape(full))
    up_shared = dot(normed[...], su[...].reshape(full))
    hidden_all[mt] = (silu(gate_shared) * up_shared).astype(BF16)
    spread(2)

    def placed(e, t):
        ids, gains = routes_all[t], gates_all[t]
        weight = jnp.where(ids[:, 0:1] == e, gains[:, 0:1], 0.0)
        weight = weight + jnp.where(ids[:, 1:2] == e, gains[:, 1:2], 0.0)
        rowsof = lax.dot_general(pick[t, e], ret[e, t], over_rows, preferred_element_type=F32)
        return weight * rowsof

    acc[mt] = placed(me, mt)

    def gather_own(k, c):
        t = lax.rem(mt + tp - k, tp)
        giveback(me, mt, me, t).wait_recv()
        acc[t] = placed(me, t)
        return c

    lax.fori_loop(1, tp, gather_own, 0)

    def gather(e):
        def one(k, c):
            t = lax.rem(mt + tp - k, tp)
            giveback(me, mt, e, t).wait_recv()
            acc[t] += placed(e, t)
            return c

        lax.fori_loop(0, tp, one, 0)

    def gather_far(j, c):
        gather(far + lax.rem(mine + j, half))
        return c

    def gather_near(j, c):
        gather(near + lax.rem(mine + j, half))
        return c

    lax.fori_loop(1, half, gather_near, 0)
    arrive(2)

    def project(t, c):
        shared[t] = dot(hidden_all[t], sd[...]).astype(BF16)
        return c

    lax.fori_loop(0, tp, project, 0)
    lax.fori_loop(0, half, gather_far, 0)

    def total(t, c):
        combined = acc[t].astype(BF16).astype(F32) + shared[t].astype(F32)
        acc[t] = combined
        squares = jnp.sum(combined * combined, axis=1, keepdims=True)
        sums[mt, t] = jnp.broadcast_to(squares, (rows, 128)).T[0:8, :]
        return c

    lax.fori_loop(0, tp, total, 0)
    spread(5)
    arrive(5)

    def finish(t, c):
        squares = sums[0, t]
        for u in range(1, tp):
            squares = squares + sums[u, t]
        squares = jnp.broadcast_to(squares[0:1, :], (128, rows)).T[:, 0:1]
        scale = lax.rsqrt(squares * (1.0 / width) + 1e-06)
        at = pl.ds(pl.multiple_of(t * rows, rows), rows)
        out[at, :] = (acc[t] * scale * post_gain[mt]).astype(BF16)
        return c

    lax.fori_loop(0, tp, finish, 0)

    def drain(d, first):
        def one(k, c):
            giveback(d, lax.rem(mt + k, tp), me, mt).wait_send()
            return c

        lax.fori_loop(first, tp, one, 0)

    def drain_far(j, c):
        d = far + lax.rem(mine + j, half)
        dispatch(d, me).wait_send()
        drain(d, 0)
        return c

    def drain_near(j, c):
        d = near + lax.rem(mine + j, half)
        dispatch(d, me).wait_send()
        drain(d, 0)
        return c

    drain(me, 1)
    lax.fori_loop(0, half, drain_far, 0)
    lax.fori_loop(1, half, drain_near, 0)

    def drain_tp(k, c):
        d = lax.rem(mt + k, tp)
        for which in range(6):
            share(which, d, mt).wait_send()
        return c

    lax.fori_loop(1, tp, drain_tp, 0)


def per_device(
    tokens, routes, gates, pre_gain, w_gate, w_up, w_down, sh_gate, sh_up, sh_down, post_gain
):
    rows, width = tokens.shape
    n = lax.axis_size("ep")
    tp = lax.axis_size("tp")
    cap = -(-max(2, 4 * rows * TOPK // (3 * n)) // 16) * 16
    lanes = -(-n // 128) * 128
    hidden = w_gate.shape[2]
    sh = sh_gate.shape[1]
    cols = width // tp
    vmem = pl.BlockSpec(memory_space=pltpu.VMEM)
    hbm = pl.BlockSpec(memory_space=pl.ANY)
    dma = pltpu.SemaphoreType.DMA
    return pl.pallas_call(
        functools.partial(kernel, n, tp, cap),
        out_shape=jax.ShapeDtypeStruct((tp * rows, cols), BF16),
        in_specs=[vmem] * 5 + [hbm] * 6,
        out_specs=vmem,
        scratch_shapes=[
            pltpu.VMEM((rows, width), BF16),
            pltpu.VMEM((tp, lanes, rows), F32),
            pltpu.VMEM((tp, n, cap, rows), BF16),
            pltpu.VMEM((n, cap, width), BF16),
            pltpu.VMEM((n, cap, width), BF16),
            pltpu.VMEM((n, tp, cap, cols), BF16),
            pltpu.VMEM((n, tp, cap, cols), BF16),
            pltpu.VMEM((width, hidden), BF16),
            pltpu.VMEM((width, hidden), BF16),
            pltpu.VMEM((hidden, width), BF16),
            pltpu.VMEM((tp, width // tp, sh), BF16),
            pltpu.VMEM((tp, width // tp, sh), BF16),
            pltpu.VMEM((sh, cols), BF16),
            pltpu.VMEM((tp, rows, cols), F32),
            pltpu.VMEM((tp, rows, cols), BF16),
            pltpu.VMEM((tp, rows, TOPK), jnp.int32),
            pltpu.VMEM((tp, rows, TOPK), F32),
            pltpu.VMEM((tp, rows, sh), BF16),
            pltpu.VMEM((tp, tp, 8, rows), F32),
            dma((6,)),
            dma((n,)), dma((n,)), dma((n, tp)), dma((n, tp)),
            dma((6, tp)), dma((6, tp)),
        ],
        compiler_params=pltpu.CompilerParams(
            collective_id=0, has_side_effects=True, vmem_limit_bytes=56 * 1024 * 1024
        ),
    )(
        tokens, routes, gates, pre_gain.reshape(1, width), post_gain.reshape(tp, 1, cols),
        w_gate, w_up, w_down, sh_gate, sh_up, sh_down,
    )


def solution(mesh):
    return jax.shard_map(
        per_device,
        mesh=mesh,
        in_specs=(
            P(("ep", "tp"), None),
            P(("ep", "tp"), None),
            P(("ep", "tp"), None),
            P(),
            P("ep", None, None),
            P("ep", None, None),
            P("ep", None, None),
            P("tp", None),
            P("tp", None),
            P(None, "tp"),
            P(),
        ),
        out_specs=P("ep", "tp"),
        check_vma=False,
    )
```

time: 119 us -> 118 us (level)
  no operation moved by 1% of the time
where the time goes in v2:
time: 118 us
  Pallas kernels  113 us (96%)
  local copies, waits for them, and re-layouts  4.94 us (4%)
    pallas_call x1, Pallas kernels, per_device(): pl.pallas_call(functools.partial(kernel, n, tp, cap), out_shape=jax.Shape...  113 us
    unnamed x3, local copies, waits for them, and re-layouts  4.94 us

profile of v2, /device:TPU:0, one launch (start us, length us, event | category | flops | bytes accessed | tf_op | source)
XLA Modules:
  0.0 117.7 jit_solution(11487895073800250699)
XLA Ops:
  0.0 1.4 %copy.12.routes = s32[192,2]{1,0:T(8,128)} copy(s32[192,2]{0,1:T(2,128)} %param.12) | data formatting | bytes 3072 | tf_op args[1]
  1.4 1.4 %copy.13.gates = f32[192,2]{1,0:T(8,128)} copy(f32[192,2]{0,1:T(2,128)} %param.13) | data formatting | bytes 3072 | tf_op args[2]
  2.9 112.7 %shard_map.109 = bf16[768,512]{1,0:T(8,128)(2,1)} custom-call(bf16[192,2048]{1,0:T(8,128)(2,1)} %tokens.1, s32[192,2]{1,0:T(8,128)} %copy.12.routes, f32[192,2]{1,0:T(8,128)} %copy.13.gates, f32[1,2048]{1,0:T(1,128)} %bitcast.2, f32[4,1,512]{2,1,0:T(1,128)} %bitcast.3, bf16[1,2048,512]{2,1,0:T(8,128)(2,1)} %w_gate.1, bf16[1,2048,512]{2,1,0:T(8,128)(2,1)} %w_up.1, ...), custom_call_target="tpu_custom_call" | custom-call | tf_op jit(solution)/shard_map/pallas_call | solution.py:352
  115.6 2.1 %copy.15 = bf16[768,512]{1,0:T(8,128)(2,1)} copy(bf16[768,512]{1,0:T(8,128)(2,1)} %shard_map.109) | data formatting | bytes 1572864

commit v3 on v2

--- a/solution.py
+++ b/solution.py
@@ -164,12 +164,15 @@
         dispatch(d, me).start()
         return c
 
-    lax.fori_loop(1, half, send_far, 0)
+    def send_both(j, c):
+        send_near(j, c)
+        return send_far(j, c)
+
+    lax.fori_loop(1, half, send_both, 0)
     spread(3)
     spread(4)
     spread(0)
     spread(1)
-    lax.fori_loop(1, half, send_near, 0)
     fill(me)
 
     for load in loads[:3]:
@@ -223,8 +226,12 @@
         serve(near + lax.rem(mine + half - j, half))
         return c
 
-    lax.fori_loop(0, half, serve_far, 0)
-    lax.fori_loop(1, half, serve_near, 0)
+    def serve_both(j, c):
+        serve_near(j, c)
+        return serve_far(j, c)
+
+    serve_far(0, 0)
+    lax.fori_loop(1, half, serve_both, 0)
 
     for load in loads[3:]:
         load.wait()

time: 118 us -> 112 us (0.949)
  Pallas kernels: 113 us -> 107 us
    pallas_call x1, Pallas kernels: 113 us -> 107 us  [per_device(): pl.pallas_call(functools.partial(kernel, n, tp, cap), out_shape=jax.Shape...]
where the time goes in v3:
time: 112 us
  Pallas kernels  107 us (96%)
  local copies, waits for them, and re-layouts  4.94 us (4%)
    pallas_call x1, Pallas kernels, per_device(): pl.pallas_call(functools.partial(kernel, n, tp, cap), out_shape=jax.Shape...  107 us
    unnamed x3, local copies, waits for them, and re-layouts  4.94 us

profile of v3, /device:TPU:0, one launch (start us, length us, event | category | flops | bytes accessed | tf_op | source)
XLA Modules:
  0.0 111.9 jit_solution(17148959498684354629)
XLA Ops:
  0.0 1.4 %copy.12.routes = s32[192,2]{1,0:T(8,128)} copy(s32[192,2]{0,1:T(2,128)} %param.12) | data formatting | bytes 3072 | tf_op args[1]
  1.4 1.4 %copy.13.gates = f32[192,2]{1,0:T(8,128)} copy(f32[192,2]{0,1:T(2,128)} %param.13) | data formatting | bytes 3072 | tf_op args[2]
  2.9 107.0 %shard_map.109 = bf16[768,512]{1,0:T(8,128)(2,1)} custom-call(bf16[192,2048]{1,0:T(8,128)(2,1)} %tokens.1, s32[192,2]{1,0:T(8,128)} %copy.12.routes, f32[192,2]{1,0:T(8,128)} %copy.13.gates, f32[1,2048]{1,0:T(1,128)} %bitcast.2, f32[4,1,512]{2,1,0:T(1,128)} %bitcast.3, bf16[1,2048,512]{2,1,0:T(8,128)(2,1)} %w_gate.1, bf16[1,2048,512]{2,1,0:T(8,128)(2,1)} %w_up.1, ...), custom_call_target="tpu_custom_call" | custom-call | tf_op jit(solution)/shard_map/pallas_call | solution.py:359
  109.8 2.1 %copy.15 = bf16[768,512]{1,0:T(8,128)(2,1)} copy(bf16[768,512]{1,0:T(8,128)(2,1)} %shard_map.109) | data formatting | bytes 1572864
